TPU v7x, 32 devices: a whole 2x2x4 slice. The times are simulated.
32 devices in a mesh: grp: 2 (over x), ep: 16 (over z, y, core).
Axes of the slice: x: 2, y: 2, z: 4, core: 2. Of those that a mesh axis runs over, the one named last changes fastest.
Arguments:
- tokens: bfloat16 [1024, 2048], P(('grp', 'ep')), parts along dimension 0, may hold values from -6 to 6
- routes: int32 [1024, 4], P(('grp', 'ep')), parts along dimension 0, may hold values from 0 to 15, all different within a row; in each aligned block of 32 rows (0 to 31, 32 to 63, ...) at most 16 rows name the same one
- route_logits: float32 [1024, 4], P(('grp', 'ep')), parts along dimension 0, may hold values from -4 to 4
- state_real: float32 [1024, 64, 64], P('grp', 'ep'), parts along dimension 0, may hold values from -4 to 4
- state_imag: float32 [1024, 64, 64], P('grp', 'ep'), parts along dimension 0, may hold values from -4 to 4
- gain_in: float32 [2048], replicated, may hold values from 0.1 to 1.9
- proj_in: bfloat16 [2048, 1024], P(None, 'ep'), may hold values from -0.125 to 0.125
- decay_rate: float32 [64, 64], P('ep'), may hold values from 0.05 to 2
- frequency: float32 [64, 64], P('ep'), may hold values from -4 to 4
- log_step: float32 [64], P('ep'), may hold values from -3 to 0
- input_real: float32 [64, 64, 16], P('ep'), may hold values from -1 to 1
- input_imag: float32 [64, 64, 16], P('ep'), may hold values from -1 to 1
- output_real: float32 [64, 16, 64], P('ep'), may hold values from -0.5 to 0.5
- output_imag: float32 [64, 16, 64], P('ep'), may hold values from -0.5 to 0.5
- skip_gain: float32 [64, 16], P('ep'), may hold values from -4 to 4
- proj_out: bfloat16 [1024, 2048], P('ep'), may hold values from -0.1875 to 0.1875
- gain_mid: float32 [2048], replicated, may hold values from 0.1 to 1.9
- expert_gate: bfloat16 [16, 2048, 1024], P('ep'), may hold values from -0.33007812 to 0.33007812
- expert_up: bfloat16 [16, 2048, 1024], P('ep'), may hold values from -0.33007812 to 0.33007812
- expert_down: bfloat16 [16, 1024, 2048], P('ep'), may hold values from -0.056152344 to 0.056152344
- dense_gate: bfloat16 [2048, 2048], P(None, 'ep'), may hold values from -0.125 to 0.125
- dense_up: bfloat16 [2048, 2048], P(None, 'ep'), may hold values from -0.125 to 0.125
- dense_down: bfloat16 [2048, 2048], P('ep'), may hold values from -0.125 to 0.125
- dense_mix: float32 [2048], P('ep'), may hold values from -0.39774758 to 0.39774758
Outputs:
- layer_out: bfloat16 [1024, 2048], P(('grp', 'ep')), parts along dimension 0
- state_real_new: float32 [1024, 64, 64], P('grp', 'ep'), parts along dimension 0
- state_imag_new: float32 [1024, 64, 64], P('grp', 'ep'), parts along dimension 0
There are 2 independent parts, one for each index of `grp`. A program takes and returns all parts, laid end to end along the dimension named above; an argument that names none is the same for every part. Nothing has to cross between parts.
Inputs may be any that keep to these rules, and one draw needn't show every extreme that they name: `routes`: each row names 4 different experts; among the rows of one device no expert is named more than 16 times, and in every draw some device names some expert exactly 16 times.
All inputs are finite; a program needn't handle non-finite values.
Results may differ from a plain program's by a relative error of at most 0.015.
Values may be sent and summed in bfloat16 or wider, within the bound.
A program may use at most 128 MiB of HBM per device.

v0:
```python
import jax
import jax.numpy as jnp
from jax import lax
from jax.sharding import PartitionSpec as P

EPS = 1e-06
LIMIT = 7.0
ALPHA = 1.702
HIGH = lax.Precision.HIGHEST


def rms_scale(values, gain_vec):
    return values * lax.rsqrt(jnp.mean(values * values, axis=-1, keepdims=True) + EPS) * gain_vec


def state_step(
    unit_rows,
    state_real,
    state_imag,
    decay_rate,
    frequency,
    log_step,
    input_real,
    input_imag,
    output_real,
    output_imag,
    skip_gain,
):
    seq_count = unit_rows.shape[0]
    groups, group_size = skip_gain.shape
    inputs = unit_rows.astype(jnp.float32).reshape(seq_count, groups, group_size)
    step_size = jnp.exp(log_step)[:, None]
    decay_part = -decay_rate
    magnitude = jnp.exp(decay_part * step_size)
    carry_real = magnitude * jnp.cos(frequency * step_size)
    carry_imag = magnitude * jnp.sin(frequency * step_size)
    denom = decay_part * decay_part + frequency * frequency
    feed_real = ((carry_real - 1.0) * decay_part + carry_imag * frequency) / denom
    feed_imag = (carry_imag * decay_part - (carry_real - 1.0) * frequency) / denom
    drive_real = jnp.einsum("sgp,gnp->sgn", inputs, input_real, precision=HIGH)
    drive_imag = jnp.einsum("sgp,gnp->sgn", inputs, input_imag, precision=HIGH)
    new_real = (
        carry_real * state_real
        - carry_imag * state_imag
        + feed_real * drive_real
        - feed_imag * drive_imag
    )
    new_imag = (
        carry_real * state_imag
        + carry_imag * state_real
        + feed_real * drive_imag
        + feed_imag * drive_real
    )
    readout = (
        jnp.einsum("gpn,sgn->sgp", output_real, new_real, precision=HIGH)
        - jnp.einsum("gpn,sgn->sgp", output_imag, new_imag, precision=HIGH)
        + skip_gain * inputs
    )
    branch = jax.nn.gelu(readout).reshape(seq_count, groups * group_size).astype(jnp.bfloat16)
    return (branch, new_real, new_imag)


def expert_apply(row_block, gate_weight, up_weight, down_weight):
    gated = jnp.minimum(jnp.dot(row_block, gate_weight, preferred_element_type=jnp.float32), LIMIT)
    upper = jnp.clip(
        jnp.dot(row_block, up_weight, preferred_element_type=jnp.float32), -LIMIT, LIMIT
    )
    activated = ((upper + 1.0) * gated * jax.nn.sigmoid(ALPHA * gated)).astype(jnp.bfloat16)
    return jnp.dot(activated, down_weight, preferred_element_type=jnp.float32).astype(jnp.bfloat16)


def dense_hidden(row_block, dense_gate, dense_up):
    return (
        jax.nn.silu(jnp.dot(row_block, dense_gate, preferred_element_type=jnp.float32))
        * jnp.dot(row_block, dense_up, preferred_element_type=jnp.float32)
    ).astype(jnp.bfloat16)


def on_device(
    tokens,
    routes,
    route_logits,
    state_real,
    state_imag,
    gain_in,
    proj_in,
    decay_rate,
    frequency,
    log_step,
    input_real,
    input_imag,
    output_real,
    output_imag,
    skip_gain,
    proj_out,
    gain_mid,
    expert_gate,
    expert_up,
    expert_down,
    dense_gate,
    dense_up,
    dense_down,
    dense_mix,
):
    devices = lax.axis_size("ep")
    own_rows = tokens.shape[0]
    top_count = routes.shape[1]
    width = tokens.shape[1]
    capacity = max(2, 2 * own_rows * top_count // devices)
    inputs = tokens.astype(jnp.float32)
    normed = rms_scale(inputs, gain_in).astype(jnp.bfloat16)
    unit_rows = jnp.dot(
        lax.all_gather(normed, "ep", axis=0, tiled=True),
        proj_in,
        preferred_element_type=jnp.float32,
    ).astype(jnp.bfloat16)
    branch, new_real, new_imag = state_step(
        unit_rows,
        state_real,
        state_imag,
        decay_rate,
        frequency,
        log_step,
        input_real,
        input_imag,
        output_real,
        output_imag,
        skip_gain,
    )
    whole_out = lax.all_gather(proj_out, "ep", axis=0, tiled=True)
    own_branch = lax.all_to_all(branch, "ep", split_axis=0, concat_axis=1, tiled=True)
    mixer_out = jnp.dot(own_branch, whole_out, preferred_element_type=jnp.float32)
    residual = inputs + mixer_out
    mixed = rms_scale(residual, gain_mid).astype(jnp.bfloat16)
    weights = jnp.exp(route_logits)
    weights = weights / jnp.sum(weights, axis=1, keepdims=True)
    hidden = dense_hidden(lax.all_gather(mixed, "ep", axis=0, tiled=True), dense_gate, dense_up)
    dense_term = jnp.dot(hidden, dense_down, preferred_element_type=jnp.float32)
    logit_term = jnp.dot(hidden.astype(jnp.float32), dense_mix, precision=HIGH)
    dense_out, gate_logit = (
        lax.psum_scatter(
            dense_term.astype(jnp.bfloat16), "ep", scatter_dimension=0, tiled=True
        ).astype(jnp.float32),
        lax.psum_scatter(
            logit_term.astype(jnp.bfloat16), "ep", scatter_dimension=0, tiled=True
        ).astype(jnp.float32),
    )
    flat_routes = routes.reshape(-1)
    chosen = (flat_routes[:, None] == jnp.arange(devices, dtype=jnp.int32)[None, :]).astype(
        jnp.int32
    )
    slot_index = jnp.sum((jnp.cumsum(chosen, axis=0) - 1) * chosen, axis=1)
    position = (flat_routes * capacity + slot_index).reshape(own_rows, top_count)
    slot_ids = jnp.arange(devices * capacity, dtype=jnp.int32)
    matches = position[:, :, None] == slot_ids[None, None, :]
    dispatch = jnp.any(matches, axis=1).astype(jnp.bfloat16)
    send_buffer = jnp.dot(dispatch.T, mixed, preferred_element_type=jnp.float32).astype(
        jnp.bfloat16
    )
    send_buffer = send_buffer.reshape(devices, capacity, width)
    received = lax.all_to_all(send_buffer, "ep", split_axis=0, concat_axis=0, tiled=True)
    flat_rows = received.reshape(-1, width)
    result = expert_apply(flat_rows, expert_gate[0], expert_up[0], expert_down[0])
    returned = lax.all_to_all(
        result.reshape(received.shape), "ep", split_axis=0, concat_axis=0, tiled=True
    )
    combine = jnp.sum(jnp.where(matches, weights[:, :, None], 0.0), axis=1)
    routed = jnp.dot(combine, returned.reshape(-1, width).astype(jnp.float32), precision=HIGH)
    layer_out = (residual + routed + jax.nn.sigmoid(gate_logit)[:, None] * dense_out).astype(
        jnp.bfloat16
    )
    return (layer_out, new_real, new_imag)


def solution(mesh):
    in_specs = (
        P(("grp", "ep"), None),
        P(("grp", "ep"), None),
        P(("grp", "ep"), None),
        P("grp", "ep", None),
        P("grp", "ep", None),
        P(),
        P(None, "ep"),
        P("ep", None),
        P("ep", None),
        P("ep"),
        P("ep", None, None),
        P("ep", None, None),
        P("ep", None, None),
        P("ep", None, None),
        P("ep", None),
        P("ep", None),
        P(),
        P("ep", None, None),
        P("ep", None, None),
        P("ep", None, None),
        P(None, "ep"),
        P(None, "ep"),
        P("ep", None),
        P("ep"),
    )
    out_specs = (P(("grp", "ep"), None), P("grp", "ep", None), P("grp", "ep", None))
    return jax.shard_map(
        on_device, mesh=mesh, in_specs=in_specs, out_specs=out_specs, check_vma=False
    )
```

profile of v0, /device:TPU:0, one launch (start us, length us, event | category | flops | bytes accessed | tf_op | source)
XLA Modules:
  0.0 239.7 jit_solution(2033976077132671135)
XLA Ops:
  7.3 1.1 fusion.38
  8.4 1.7 fusion.40
  10.1 0.0 all-gather.6.cloned.1.call-start
  10.2 0.7 all-gather.6.cloned.1.call-update
  10.9 0.0 all-gather.8.cloned.1.call-start
  10.9 0.7 exp.19
  11.6 0.8 cosine_multiply_fusion
  12.4 42.6 %all-gather.4.cloned.1.call-done = bf16[512,2048]{1,0:T(8,128)(2,1)} async-done(((bf16[32,2048]{1,0:T(8,128)(2,1)}), bf16[512,2048]{1,0:T(8,128)(2,1)}) %all-gather.4.cloned.1.call-update) | async-done | bytes 2097168 | tf_op jit(solution)/shard_map/all_gather | solution.py:113
  55.0 2.3 convolution_convert_fusion.2
  57.3 1.2 fusion.59
  58.5 1.3 bitcast_add_fusion
  59.9 0.4 fusion.60
  60.4 0.4 fusion.48
  60.8 0.2 convert_element_type.57
  61.0 0.3 copy.48
  61.3 0.1 reshape.75
  61.4 11.5 %all_to_all.26 = bf16[16,2,1024]{2,1,0:T(2,128)(2,1)S(1)} all-to-all(bf16[16,2,1024]{2,1,0:T(2,128)(2,1)S(1)} %reshape.75), channel_id=1, replica_groups=mesh['grp'=2,'ep'=16] {'ep'}, dimensions={0} | all-to-all | bytes 131072 | tf_op jit(solution)/shard_map/all_to_all | solution.py:131
  72.9 0.1 reshape.76
  73.0 0.1 copy.49
  73.1 0.1 all_to_all.20
  73.2 34.4 %all-gather.6.cloned.1.call-done = bf16[1024,2048]{1,0:T(8,128)(2,1)} async-done(((bf16[64,2048]{1,0:T(8,128)(2,1)}), bf16[1024,2048]{1,0:T(8,128)(2,1)}) %all-gather.6.cloned.1.call-update) | async-done | bytes 4194320 | tf_op jit(solution)/shard_map/all_gather | solution.py:130
  107.6 3.1 %multiply_reduce_fusion = (f32[32]{0:T(128)S(1)}, f32[32,2048]{1,0:T(8,128)S(1)}) fusion(bf16[32,1024]{1,0:T(8,128)(2,1)S(1)} %all_to_all.20, bf16[1024,2048]{1,0:T(8,128)(2,1)} %all-gather.6.cloned.1.call-done, bf16[32,2048]{1,0:T(8,128)(2,1)S(1)} %copy-done.3), kind=kOutput, calls=%fused_computation.39 | convolution fusion | flops 134479840 | bytes 4653184 | tf_op jit(solution)/shard_map/dot_general | solution.py:132
  110.8 0.7 multiply_convert_fusion
  111.6 0.1 copy.50
  111.6 0.1 eq.28
  111.8 0.1 fusion.50
  111.9 0.2 reduce_window_sum.11
  112.0 0.2 select_reduce_fusion.1
  112.2 0.1 reduce_sum.49
  112.3 0.1 copy.51
  112.4 0.1 fusion.49
  112.5 2.4 convolution_convert_fusion.1
  114.9 3.7 %all-to-all-start.1 = ((bf16[16,16,2048]{2,1,0:T(8,128)(2,1)}), bf16[16,16,2048]{2,1,0:T(8,128)(2,1)S(1)}, u32[]{:S(2)}, u32[]{:S(2)}) async-start(bf16[16,16,2048]{2,1,0:T(8,128)(2,1)} %bitcast.7), calls=%async_computation.1 | async-start | bytes 2097152 | tf_op jit(solution)/shard_map/all_to_all | solution.py:161
  118.5 0.0 reduce-scatter.2.cloned.1.call-start
  118.6 40.5 %all-gather.8.cloned.1.call-done = bf16[512,2048]{1,0:T(8,128)(2,1)} async-done(((bf16[32,2048]{1,0:T(8,128)(2,1)}), bf16[512,2048]{1,0:T(8,128)(2,1)}) %all-gather.8.cloned.1.call-update) | async-done | bytes 2097168 | tf_op jit(solution)/shard_map/all_gather | solution.py:137
  159.1 2.3 fusion.61
  161.4 2.3 fusion.29
  163.7 2.0 convolution_convert_fusion
  165.8 3.5 %fusion.11 = f32[256,1024]{1,0:T(8,128)S(1)} fusion(bf16[256,2048]{1,0:T(8,128)(2,1)S(1)} %bitcast.87, bf16[1,2048,1024]{2,1,0:T(8,128)(2,1)} %param.41), kind=kOutput, calls=%fused_computation.13 | convolution fusion | flops 1074003968 | bytes 6291456 | tf_op jit(solution)/shard_map/dot_general | solution.py:64
  169.3 7.2 %fusion.6 = bf16[256,2048]{1,0:T(8,128)(2,1)} fusion(bf16[1,1024,2048]{2,1,0:T(8,128)(2,1)} %param.43, f32[256,1024]{1,0:T(8,128)S(1)} %fusion.11, bf16[256,2048]{1,0:T(8,128)(2,1)S(1)} %bitcast.88, bf16[1,2048,1024]{2,1,0:T(8,128)(2,1)} %param.42), kind=kOutput, calls=%fused_computation.7 | convolution fusion | flops 2150367232 | bytes 11534336 | tf_op jit(solution)/shard_map/dot_general | solution.py:69
  176.5 3.7 %all-to-all-start.2 = ((bf16[16,16,2048]{2,1,0:T(8,128)(2,1)}), bf16[16,16,2048]{2,1,0:T(8,128)(2,1)S(1)}, u32[]{:S(2)}, u32[]{:S(2)}) async-start(bf16[16,16,2048]{2,1,0:T(8,128)(2,1)} %bitcast.12), calls=%async_computation.2 | async-start | bytes 2097152 | tf_op jit(solution)/shard_map/all_to_all | solution.py:164
  180.2 0.6 dynamic-slice
  181.4 0.1 select_reduce_fusion
  181.6 0.2 fusion.53
  181.8 47.0 %all-reduce = bf16[512]{0:T(512)(128)(2,1)S(1)} all-reduce(bf16[512]{0:T(512)(128)(2,1)S(1)} %convert_element_type.64), channel_id=2, replica_groups=mesh['grp'=2,'ep'=16] {'ep'}, use_global_device_ids=true, to_apply=%region_7.8.clone | all-reduce | flops 512 | bytes 2048
  228.7 0.1 add_divide_fusion.1
  228.8 2.1 reduce-scatter.2.cloned.1.call-done
  231.0 2.2 fusion.10
  (44 shorter events, 0.2 us)
Async XLA Ops:
  7.2 156.5 %copy-start = (bf16[128,2048]{1,0:T(8,128)(2,1)S(1)}, bf16[128,2048]{1,0:T(8,128)(2,1)}, u32[]{:S(2)}) copy-start(bf16[128,2048]{1,0:T(8,128)(2,1)} %param.46) | copy-start | bytes 1572868
  7.2 51.3 %copy-start.4 = (f32[512,4,64]{0,2,1:T(8,128)S(1)}, f32[512,4,64]{0,2,1:T(8,128)}, u32[]{:S(2)}) copy-start(f32[512,4,64]{0,2,1:T(8,128)} %param.27) | copy-start | bytes 1572868
  7.2 51.3 %copy-start.5 = (f32[512,4,64]{0,2,1:T(8,128)S(1)}, f32[512,4,64]{0,2,1:T(8,128)}, u32[]{:S(2)}) copy-start(f32[512,4,64]{0,2,1:T(8,128)} %param.28) | copy-start | bytes 1572868
  7.2 52.7 %copy-start.8 = (f32[4,16,64]{2,1,0:T(8,128)S(1)}, f32[4,16,64]{2,1,0:T(8,128)}, u32[]{:S(2)}) copy-start(f32[4,16,64]{2,1,0:T(8,128)} %param.36) | copy-start | bytes 49156
  7.2 53.1 %copy-start.7 = (f32[4,16,64]{2,1,0:T(8,128)S(1)}, f32[4,16,64]{2,1,0:T(8,128)}, u32[]{:S(2)}) copy-start(f32[4,16,64]{2,1,0:T(8,128)} %param.37) | copy-start | bytes 49156
  7.2 53.1 %copy-start.12 = (f32[4,16]{1,0:T(4,128)S(1)}, f32[4,16]{1,0:T(4,128)}, u32[]{:S(2)}) copy-start(f32[4,16]{1,0:T(4,128)} %param.38) | copy-start | bytes 772
  7.2 47.8 %all-gather.4.cloned.1.call-start = ((), (), s32[]{:S(2)}) async-start(), calls=%async_computation.4 | async-start | bytes 2228224 | tf_op jit(solution)/shard_map/all_gather | solution.py:113
  10.1 97.5 %all-gather.6.cloned.1.call-start = ((), (), s32[]{:S(2)}) async-start(), calls=%async_computation.5 | async-start | bytes 4456448 | tf_op jit(solution)/shard_map/all_gather | solution.py:130
  10.9 148.2 %all-gather.8.cloned.1.call-start = ((), (), s32[]{:S(2)}) async-start(), calls=%async_computation.6 | async-start | bytes 2228224 | tf_op jit(solution)/shard_map/all_gather | solution.py:137
  12.4 95.2 %copy-start.3 = (bf16[32,2048]{1,0:T(8,128)(2,1)S(1)}, bf16[32,2048]{1,0:T(8,128)(2,1)}, u32[]{:S(2)}) copy-start(bf16[32,2048]{1,0:T(8,128)(2,1)} %param.24) | copy-start | bytes 393220
  59.9 51.6 %copy-start.1 = (f32[512,4,64]{0,2,1:T(8,128)}, f32[512,4,64]{0,2,1:T(8,128)S(1)}, u32[]{:S(2)}) copy-start(f32[512,4,64]{0,2,1:T(8,128)S(1)} %get-tuple-element.3) | copy-start | bytes 1572868
  59.9 51.6 %copy-start.2 = (f32[512,4,64]{0,2,1:T(8,128)}, f32[512,4,64]{0,2,1:T(8,128)S(1)}, u32[]{:S(2)}) copy-start(f32[512,4,64]{0,2,1:T(8,128)S(1)} %get-tuple-element.4) | copy-start | bytes 1572868
  59.9 50.8 %copy-start.9 = (f32[2048]{0:T(1024)S(1)}, f32[2048]{0:T(1024)}, u32[]{:S(2)}) copy-start(f32[2048]{0:T(1024)} %param.40) | copy-start | bytes 24580
  59.9 51.6 %copy-start.10 = (s32[32,4]{0,1:T(4,128)S(1)}, s32[32,4]{0,1:T(4,128)}, u32[]{:S(2)}) copy-start(s32[32,4]{0,1:T(4,128)} %param.25) | copy-start | bytes 1540
  73.2 85.8 %copy-start.6 = (bf16[2048,128]{1,0:T(8,128)(2,1)S(1)}, bf16[2048,128]{1,0:T(8,128)(2,1)}, u32[]{:S(2)}) copy-start(bf16[2048,128]{1,0:T(8,128)(2,1)} %param.44) | copy-start | bytes 1572868
  110.7 50.6 %copy-start.14 = (bf16[2048,128]{1,0:T(8,128)(2,1)S(1)}, bf16[2048,128]{1,0:T(8,128)(2,1)}, u32[]{:S(2)}) copy-start(bf16[2048,128]{1,0:T(8,128)(2,1)} %param.45) | copy-start | bytes 1572868
  114.9 50.9 %all-to-all-start.1 = ((bf16[16,16,2048]{2,1,0:T(8,128)(2,1)}), bf16[16,16,2048]{2,1,0:T(8,128)(2,1)S(1)}, u32[]{:S(2)}, u32[]{:S(2)}) async-start(bf16[16,16,2048]{2,1,0:T(8,128)(2,1)} %bitcast.7), calls=%async_computation.1 | async-start | bytes 2097152 | tf_op jit(solution)/shard_map/all_to_all | solution.py:161
  118.5 112.4 %reduce-scatter.2.cloned.1.call-start = ((), (), s32[]{:S(2)}) async-start(), calls=%async_computation.7 | async-start | bytes 2228224 | tf_op jit(solution)/shard_map/reduce_scatter | solution.py:141
  169.2 10.9 %copy-start.15 = (u32[32]{0:T(128)S(1)}, u32[32]{0:T(128)}, u32[]{:S(2)}) copy-start(u32[32]{0:T(128)} %constant.58) | copy-start | bytes 388
  169.2 12.2 %copy-start.11 = (f32[32,4]{0,1:T(4,128)S(1)}, f32[32,4]{0,1:T(4,128)}, u32[]{:S(2)}) copy-start(f32[32,4]{0,1:T(4,128)} %param.26) | copy-start | bytes 1540
  169.3 12.3 %copy-start.13 = (f32[128]{0:T(128)S(1)}, f32[128]{0:T(128)}, u32[]{:S(2)}) copy-start(f32[128]{0:T(128)} %param.47) | copy-start | bytes 1540
  176.5 52.3 %all-to-all-start.2 = ((bf16[16,16,2048]{2,1,0:T(8,128)(2,1)}), bf16[16,16,2048]{2,1,0:T(8,128)(2,1)S(1)}, u32[]{:S(2)}, u32[]{:S(2)}) async-start(bf16[16,16,2048]{2,1,0:T(8,128)(2,1)} %bitcast.12), calls=%async_computation.2 | async-start | bytes 2097152 | tf_op jit(solution)/shard_map/all_to_all | solution.py:164
Sparse Core Ops, SparseCore 0:
  10.8 44.1 all-gather.3
  57.1 50.3 all-gather.5
  111.7 47.3 all-gather.7
  165.9 65.0 reduce-scatter.1
where the time goes:
time: 240 us
  waiting for transfers between devices  120 us (50%)
  blocking collectives  58.4 us (24%)
  matrix products  30.9 us (13%)
  between operations  14.8 us (6%)
  starting transfers between devices  7.47 us (3%)
  other arithmetic  5.14 us (2%)
  local copies, waits for them, and re-layouts  2.64 us (1%)
    unnamed x1, blocking collectives  47 us
    all_gather x1, waiting for transfers between devices, on_device(): lax.all_gather(normed, 'ep', axis=0, tiled=True)  42.6 us
    all_gather x1, waiting for transfers between devices, on_device(): lax.all_gather(mixed, 'ep', axis=0, tiled=True)  40.5 us
    all_gather x1, waiting for transfers between devices, on_device(): whole_out = lax.all_gather(proj_out, 'ep', axis=0, tiled=True)  34.4 us
    all_to_all x1, blocking collectives, on_device(): lax.all_to_all(branch, 'ep', split_axis=0, concat_axis=1, tiled=True)  11.5 us
    dot_general x1, matrix products, expert_apply(): jnp.dot(activated, down_weight, preferred_element_type=jnp.float32)  7.23 us
  transfers between devices with their start and end apart: 6, of which 4 were waited for; matrix products, arithmetic and copies ran while one was open for 12% of the time, Pallas kernels for 0%

commit v1 on v0

--- a/solution.py
+++ b/solution.py
@@ -1,6 +1,10 @@
+import functools
+
 import jax
 import jax.numpy as jnp
 from jax import lax
+from jax.experimental import pallas as pl
+from jax.experimental.pallas import tpu as pltpu
 from jax.sharding import PartitionSpec as P
 
 EPS = 1e-06
@@ -69,6 +73,213 @@
     return jnp.dot(activated, down_weight, preferred_element_type=jnp.float32).astype(jnp.bfloat16)
 
 
+def spot(n):
+    me = lax.axis_index("ep")
+    return me, me // 4, (me // 2) % 2, me % 2, n // 4
+
+
+def index_of(hi, mid, lo):
+    return hi * 4 + mid * 2 + lo
+
+
+def greet(peers):
+    barrier = pltpu.get_barrier_semaphore()
+    for peer in peers:
+        pl.semaphore_signal(
+            barrier, inc=1, device_id={"ep": peer}, device_id_type=pl.DeviceIdType.MESH
+        )
+    pl.semaphore_wait(barrier, len(peers))
+
+
+def remote(src, dst, send_sem, recv_sem, peer):
+    return pltpu.make_async_remote_copy(
+        src_ref=src,
+        dst_ref=dst,
+        send_sem=send_sem,
+        recv_sem=recv_sem,
+        device_id={"ep": peer},
+        device_id_type=pl.DeviceIdType.MESH,
+    )
+
+
+def gather_kernel(n, x_ref, o_ref, send_sem, z_sem, y_sem, c_sem):
+    me, hi, mid, lo, span = spot(n)
+    core = index_of(hi, mid, 1 - lo)
+    across = index_of(hi, 1 - mid, lo)
+    ahead = [(hi + 1 + j) % span for j in range(span - 1)]
+    behind = [(hi + span - 1 - j) % span for j in range(span - 1)]
+    greet([core, across] + [index_of(h, mid, lo) for h in ahead])
+    sent = []
+
+    def push(src, slot, sem, peer):
+        copy = remote(src, o_ref.at[slot], send_sem.at[len(sent)], sem, peer)
+        copy.start()
+        sent.append(copy)
+        return copy
+
+    z_copies = [
+        push(x_ref, me, z_sem.at[j], index_of(ahead[j], mid, lo)) for j in range(span - 1)
+    ]
+    y_copies = [push(x_ref, me, y_sem.at[0], across)]
+    c_copies = [push(x_ref, me, c_sem.at[0], core)]
+    o_ref[me] = x_ref[...]
+    for j in range(span):
+        if j < span - 1:
+            z_copies[j].wait_recv()
+            slot = index_of(behind[j], mid, lo)
+            y_copies.append(push(o_ref.at[slot], slot, y_sem.at[j + 1], across))
+            c_copies.append(push(o_ref.at[slot], slot, c_sem.at[j + 1], core))
+        y_copies[j].wait_recv()
+        slot = index_of(hi if j == 0 else behind[j - 1], 1 - mid, lo)
+        c_copies.append(push(o_ref.at[slot], slot, c_sem.at[span + j], core))
+    for copy in c_copies:
+        copy.wait_recv()
+    for copy in sent:
+        copy.wait_send()
+
+
+def gather_rows(x, n, collective_id):
+    rows, width = x.shape
+    span = n // 4
+    out = pl.pallas_call(
+        functools.partial(gather_kernel, n),
+        out_shape=jax.ShapeDtypeStruct((n, rows, width), x.dtype),
+        in_specs=[pl.BlockSpec(memory_space=pltpu.VMEM)],
+        out_specs=pl.BlockSpec(memory_space=pltpu.VMEM),
+        scratch_shapes=[
+            pltpu.SemaphoreType.DMA((4 * span,)),
+            pltpu.SemaphoreType.DMA((span,)),
+            pltpu.SemaphoreType.DMA((span,)),
+            pltpu.SemaphoreType.DMA((2 * span,)),
+        ],
+        compiler_params=pltpu.CompilerParams(
+            collective_id=collective_id, has_side_effects=True
+        ),
+        name=f"gather_{collective_id}",
+    )(x)
+    return out.reshape(n * rows, width)
+
+
+def scatter_kernel(
+    n, x_ref, o_ref, c_buf, y_out, y_buf, z_out, z_buf, send_sem, c_sem, y_sem, z_sem
+):
+    me, hi, mid, lo, span = spot(n)
+    core = index_of(hi, mid, 1 - lo)
+    across = index_of(hi, 1 - mid, lo)
+    order = [(hi + 1 + j) % span for j in range(span)]
+    greet([core, across] + [index_of(h, mid, lo) for h in order[:-1]])
+    sent = []
+
+    def push(src, dst, sem, peer):
+        copy = remote(src, dst, send_sem.at[len(sent)], sem, peer)
+        copy.start()
+        sent.append(copy)
+        return copy
+
+    c_copies = []
+    for turn, side in enumerate((1 - mid, mid)):
+        for j in range(span):
+            at = turn * span + j
+            c_copies.append(
+                push(
+                    x_ref.at[index_of(order[j], side, 1 - lo)], c_buf.at[at], c_sem.at[at], core
+                )
+            )
+    y_copies = []
+    for j in range(span):
+        c_copies[j].wait_recv()
+        own = x_ref[index_of(order[j], 1 - mid, lo)].astype(jnp.float32)
+        y_out[j] = (own + c_buf[j].astype(jnp.float32)).astype(y_out.dtype)
+        y_copies.append(push(y_out.at[j], y_buf.at[j], y_sem.at[j], across))
+    z_copies = []
+    total = None
+    for j in range(span):
+        c_copies[span + j].wait_recv()
+        y_copies[j].wait_recv()
+        value = (
+            x_ref[index_of(order[j], mid, lo)].astype(jnp.float32)
+            + c_buf[span + j].astype(jnp.float32)
+            + y_buf[j].astype(jnp.float32)
+        )
+        if j < span - 1:
+            z_out[j] = value.astype(z_out.dtype)
+            z_copies.append(
+                push(z_out.at[j], z_buf.at[j], z_sem.at[j], index_of(order[j], mid, lo))
+            )
+        else:
+            o_ref[...] = value
+    for j in range(span - 1):
+        z_copies[j].wait_recv()
+        o_ref[...] += z_buf[j].astype(jnp.float32)
+    for copy in sent:
+        copy.wait_send()
+
+
+def scatter_rows(x, n, collective_id):
+    rows, width = x.shape[0] // n, x.shape[1]
+    span = n // 4
+    block = (rows, width)
+    return pl.pallas_call(
+        functools.partial(scatter_kernel, n),
+        out_shape=jax.ShapeDtypeStruct(block, jnp.float32),
+        in_specs=[pl.BlockSpec(memory_space=pltpu.VMEM)],
+        out_specs=pl.BlockSpec(memory_space=pltpu.VMEM),
+        scratch_shapes=[
+            pltpu.VMEM((2 * span,) + block, x.dtype),
+            pltpu.VMEM((span,) + block, x.dtype),
+            pltpu.VMEM((span,) + block, x.dtype),
+            pltpu.VMEM((span,) + block, x.dtype),
+            pltpu.VMEM((span,) + block, x.dtype),
+            pltpu.SemaphoreType.DMA((4 * span,)),
+            pltpu.SemaphoreType.DMA((2 * span,)),
+            pltpu.SemaphoreType.DMA((span,)),
+            pltpu.SemaphoreType.DMA((span,)),
+        ],
+        compiler_params=pltpu.CompilerParams(
+            collective_id=collective_id, has_side_effects=True
+        ),
+        name=f"scatter_{collective_id}",
+    )(x.reshape((n,) + block))
+
+
+def total_kernel(n, x_ref, o_ref, buf, send_sem, recv_sem):
+    me = lax.axis_index("ep")
+    peers = [(me + 1 + j) % n for j in range(n - 1)]
+    greet(peers)
+    copies = [
+        remote(x_ref, buf.at[j], send_sem.at[j], recv_sem.at[j], peers[j]) for j in range(n - 1)
+    ]
+    for copy in copies:
+        copy.start()
+    value = x_ref[...]
+    for j in range(n - 1):
+        copies[j].wait_recv()
+        value = value + buf[j]
+    o_ref[...] = value
+    for copy in copies:
+        copy.wait_send()
+
+
+def total_over(x, n, collective_id):
+    lanes = x.reshape(-1, 128)
+    out = pl.pallas_call(
+        functools.partial(total_kernel, n),
+        out_shape=jax.ShapeDtypeStruct(lanes.shape, lanes.dtype),
+        in_specs=[pl.BlockSpec(memory_space=pltpu.VMEM)],
+        out_specs=pl.BlockSpec(memory_space=pltpu.VMEM),
+        scratch_shapes=[
+            pltpu.VMEM((n - 1,) + lanes.shape, lanes.dtype),
+            pltpu.SemaphoreType.DMA((n - 1,)),
+            pltpu.SemaphoreType.DMA((n - 1,)),
+        ],
+        compiler_params=pltpu.CompilerParams(
+            collective_id=collective_id, has_side_effects=True
+        ),
+        name=f"total_{collective_id}",
+    )(lanes)
+    return out.reshape(x.shape)
+
+
 def dense_hidden(row_block, dense_gate, dense_up):
     return (
         jax.nn.silu(jnp.dot(row_block, dense_gate, preferred_element_type=jnp.float32))
@@ -103,16 +314,14 @@
     dense_mix,
 ):
     devices = lax.axis_size("ep")
-    own_rows = tokens.shape[0]
+    me = lax.axis_index("ep")
+    own_rows, width = tokens.shape
     top_count = routes.shape[1]
-    width = tokens.shape[1]
     capacity = max(2, 2 * own_rows * top_count // devices)
     inputs = tokens.astype(jnp.float32)
     normed = rms_scale(inputs, gain_in).astype(jnp.bfloat16)
     unit_rows = jnp.dot(
-        lax.all_gather(normed, "ep", axis=0, tiled=True),
-        proj_in,
-        preferred_element_type=jnp.float32,
+        gather_rows(normed, devices, 0), proj_in, preferred_element_type=jnp.float32
     ).astype(jnp.bfloat16)
     branch, new_real, new_imag = state_step(
         unit_rows,
@@ -127,48 +336,43 @@
         output_imag,
         skip_gain,
     )
-    whole_out = lax.all_gather(proj_out, "ep", axis=0, tiled=True)
-    own_branch = lax.all_to_all(branch, "ep", split_axis=0, concat_axis=1, tiled=True)
-    mixer_out = jnp.dot(own_branch, whole_out, preferred_element_type=jnp.float32)
-    residual = inputs + mixer_out
+    mixer_part = jnp.dot(branch, proj_out, preferred_element_type=jnp.float32)
+    residual = inputs + scatter_rows(mixer_part.astype(jnp.bfloat16), devices, 1)
     mixed = rms_scale(residual, gain_mid).astype(jnp.bfloat16)
     weights = jnp.exp(route_logits)
     weights = weights / jnp.sum(weights, axis=1, keepdims=True)
-    hidden = dense_hidden(lax.all_gather(mixed, "ep", axis=0, tiled=True), dense_gate, dense_up)
+    expert_ids = jnp.arange(devices, dtype=jnp.int32)
+    named = routes[:, :, None] == expert_ids[None, None, :]
+    table = jnp.sum(jnp.where(named, weights[:, :, None], 0.0), axis=1)
+    coarse = table.astype(jnp.bfloat16)
+    fine = (table - coarse.astype(jnp.float32)).astype(jnp.bfloat16)
+    spare = jnp.zeros((own_rows, -(2 * devices) % 128), jnp.bfloat16)
+    gathered = gather_rows(jnp.concatenate([mixed, coarse, fine, spare], axis=1), devices, 2)
+    all_mixed = gathered[:, :width]
+    hidden = dense_hidden(all_mixed, dense_gate, dense_up)
+    logit_term = jnp.dot(hidden.astype(jnp.float32), dense_mix, precision=HIGH)
+    gate_logit = total_over(logit_term, devices, 3)
     dense_term = jnp.dot(hidden, dense_down, preferred_element_type=jnp.float32)
-    logit_term = jnp.dot(hidden.astype(jnp.float32), dense_mix, precision=HIGH)
-    dense_out, gate_logit = (
-        lax.psum_scatter(
-            dense_term.astype(jnp.bfloat16), "ep", scatter_dimension=0, tiled=True
-        ).astype(jnp.float32),
-        lax.psum_scatter(
-            logit_term.astype(jnp.bfloat16), "ep", scatter_dimension=0, tiled=True
-        ).astype(jnp.float32),
-    )
-    flat_routes = routes.reshape(-1)
-    chosen = (flat_routes[:, None] == jnp.arange(devices, dtype=jnp.int32)[None, :]).astype(
-        jnp.int32
-    )
-    slot_index = jnp.sum((jnp.cumsum(chosen, axis=0) - 1) * chosen, axis=1)
-    position = (flat_routes * capacity + slot_index).reshape(own_rows, top_count)
+    mine = (expert_ids == me)[None, :]
+    extra = gathered[:, width:].astype(jnp.float32)
+    share = jnp.sum(
+        jnp.where(mine, extra[:, :devices] + extra[:, devices : 2 * devices], 0.0), axis=1
+    ).reshape(devices, own_rows)
+    taken = share > 0.0
+    slot = jnp.cumsum(taken.astype(jnp.int32), axis=1) - 1
+    slot = jnp.where(taken, slot + expert_ids[:, None] * capacity, -1).reshape(-1)
     slot_ids = jnp.arange(devices * capacity, dtype=jnp.int32)
-    matches = position[:, :, None] == slot_ids[None, None, :]
-    dispatch = jnp.any(matches, axis=1).astype(jnp.bfloat16)
-    send_buffer = jnp.dot(dispatch.T, mixed, preferred_element_type=jnp.float32).astype(
-        jnp.bfloat16
-    )
-    send_buffer = send_buffer.reshape(devices, capacity, width)
-    received = lax.all_to_all(send_buffer, "ep", split_axis=0, concat_axis=0, tiled=True)
-    flat_rows = received.reshape(-1, width)
+    picks = slot[None, :] == slot_ids[:, None]
+    places = slot[:, None] == slot_ids[None, :]
+    flat_rows = jnp.dot(
+        picks.astype(jnp.bfloat16), all_mixed, preferred_element_type=jnp.float32
+    ).astype(jnp.bfloat16)
     result = expert_apply(flat_rows, expert_gate[0], expert_up[0], expert_down[0])
-    returned = lax.all_to_all(
-        result.reshape(received.shape), "ep", split_axis=0, concat_axis=0, tiled=True
-    )
-    combine = jnp.sum(jnp.where(matches, weights[:, :, None], 0.0), axis=1)
-    routed = jnp.dot(combine, returned.reshape(-1, width).astype(jnp.float32), precision=HIGH)
-    layer_out = (residual + routed + jax.nn.sigmoid(gate_logit)[:, None] * dense_out).astype(
-        jnp.bfloat16
-    )
+    slot_share = jnp.sum(jnp.where(picks, share.reshape(1, -1), 0.0), axis=1, keepdims=True)
+    scaled = (result.astype(jnp.float32) * slot_share).astype(jnp.bfloat16)
+    routed = jnp.dot(places.astype(jnp.bfloat16), scaled, preferred_element_type=jnp.float32)
+    part = (routed + jax.nn.sigmoid(gate_logit)[:, None] * dense_term).astype(jnp.bfloat16)
+    layer_out = (residual + scatter_rows(part, devices, 4)).astype(jnp.bfloat16)
     return (layer_out, new_real, new_imag)
 
 

time: 240 us -> 148 us (0.62)
  waiting for transfers between devices: 120 us -> 0 us
  Pallas kernels: 0 us -> 107 us
  blocking collectives: 58.4 us -> 0 us
  between operations: 14.8 us -> 1.02 us
  starting transfers between devices: 7.47 us -> 0 us
  other arithmetic: 5.14 us -> 10.8 us
  matrix products: 30.9 us -> 26.2 us
    all_gather x3 -> x0, waiting for transfers between devices: 117 us -> none  [the longest x1 42.6 us: on_device(): lax.all_gather(normed, 'ep', axis=0, tiled=True)]
    pallas_call x0 -> x5, Pallas kernels: none -> 107 us  [the longest x2 49.4 us: scatter_rows(): pl.pallas_call(functools.partial(scatter_kernel, n), out_shape=jax.ShapeD...]
    unnamed x1 -> x0, blocking collectives: 47 us -> none
    all_to_all x1 -> x0, blocking collectives: 11.5 us -> none  [on_device(): lax.all_to_all(branch, 'ep', split_axis=0, concat_axis=1, tiled=True)]
    all_to_all x2 -> x0, starting transfers between devices: 7.31 us -> none  [the longest x1 3.65 us: on_device(): lax.all_to_all(result.reshape(received.shape), 'ep', split_axis=0, concat...]
    dot_general x5, matrix products: 17.2 us -> 12.5 us  [the longest x1 5.93 us: on_device(): jnp.dot(places.astype(jnp.bfloat16), scaled, preferred_element_type=jnp.f...]
  transfers between devices with their start and end apart: 6 -> 0, of which waited for: 4 -> 0; matrix products, arithmetic and copies ran while one was open for 12% -> 0% of each run, Pallas kernels for 0% -> 0%
where the time goes in v1:
time: 148 us; the launch traced here: 147 us
  Pallas kernels  107 us (72%)
  matrix products  26.2 us (18%)
  other arithmetic  10.8 us (7%)
  local copies, waits for them, and re-layouts  1.96 us (1%)
    pallas_call x2, Pallas kernels, scatter_rows(): pl.pallas_call(functools.partial(scatter_kernel, n), out_shape=jax.ShapeD...  49.4 us
    pallas_call x2, Pallas kernels, gather_rows(): pl.pallas_call(functools.partial(gather_kernel, n), out_shape=jax.ShapeDt...  49.3 us
    pallas_call x1, Pallas kernels, total_over(): pl.pallas_call(functools.partial(total_kernel, n), out_shape=jax.ShapeDty...  8.56 us
    dot_general x1, matrix products, on_device(): jnp.dot(places.astype(jnp.bfloat16), scaled, preferred_element_type=jnp.f...  5.93 us
    dot_general x1, matrix products, on_device(): dense_term = jnp.dot(hidden, dense_down, preferred_element_type=jnp.float32)  4.21 us
    dot_general x1, matrix products, expert_apply(): jnp.dot(row_block, gate_weight, preferred_element_type=jnp.float32)  3.63 us

profile of v1, /device:TPU:0, one launch (start us, length us, event | category | flops | bytes accessed | tf_op | source)
XLA Modules:
  0.0 147.2 jit_solution(6889065693004540349)
XLA Ops:
  0.6 0.0 copy-start
  0.7 0.7 exp.24
  1.4 0.7 exponential_reduce_fusion
  2.1 1.0 fusion.53
  3.2 0.7 exponential_divide_fusion
  3.9 0.7 select_reduce_fusion.1
  4.6 0.1 copy.33
  4.7 0.8 cosine_multiply_fusion
  5.5 0.1 copy.32
  5.6 1.7 %fusion.55.x_ref = bf16[32,2048]{1,0:T(8,128)(2,1)} fusion(bf16[32,2048]{1,0:T(8,128)(2,1)} %param.24, f32[2048]{0:T(1024)} %param.29, f32[32]{0:T(128)S(1)} %add_rsqrt_fusion.1), kind=kLoop, calls=%fused_computation.44 | loop fusion | flops 262144 | bytes 270464 | tf_op jit(solution)/shard_map/convert_element_type | solution.py:322
  7.2 25.7 %gather_0.1 = bf16[16,32,2048]{2,1,0:T(8,128)(2,1)} custom-call(bf16[32,2048]{1,0:T(8,128)(2,1)} %fusion.55.x_ref), custom_call_target="tpu_custom_call" | custom-call | tf_op jit(solution)/shard_map/gather_0/pallas_call | solution.py:144
  33.0 2.3 %convolution_convert_fusion.2 = bf16[512,64]{0,1:T(8,128)(2,1)S(1)} fusion(bf16[512,2048]{1,0:T(8,128)(2,1)} %bitcast.87, bf16[2048,64]{0,1:T(8,128)(2,1)S(1)} %copy-done.8), kind=kOutput, calls=%fused_computation.30 | convolution fusion | flops 134250496 | bytes 2424832 | tf_op jit(solution)/shard_map/dot_general | solution.py:323
  35.4 0.0 copy-start.12
  35.4 0.0 copy-start.15
  35.4 0.4 fusion.71
  35.8 0.0 copy-start.9
  35.9 0.6 bitcast_add_fusion
  36.4 0.0 copy-start.4
  36.4 0.0 copy-start.5
  36.5 0.4 fusion.72
  36.9 0.4 fusion.67
  37.3 0.1 copy-done.5
  37.4 2.1 %convolution_convert_fusion = bf16[512,2048]{1,0:T(8,128)(2,1)} fusion(bf16[512,64]{0,1:T(8,128)(2,1)S(1)} %bitcast.95, bf16[64,2048]{1,0:T(8,128)(2,1)S(1)} %copy-done.9), kind=kOutput, calls=%fused_computation.7 | convolution fusion | flops 135266304 | bytes 2424832 | tf_op jit(solution)/shard_map/dot_general | solution.py:339
  39.5 25.1 %scatter_1.1 = f32[32,2048]{1,0:T(8,128)} custom-call(bf16[16,32,2048]{2,1,0:T(8,128)(2,1)} %bitcast.85), custom_call_target="tpu_custom_call" | custom-call | tf_op jit(solution)/shard_map/scatter_1/pallas_call | solution.py:222
  64.6 1.1 multiply_reduce_fusion
  65.7 1.0 multiply_convert_fusion
  66.7 0.7 concatenate.3.x_ref
  67.5 23.5 %gather_2.1 = bf16[16,32,2176]{2,1,0:T(8,128)(2,1)} custom-call(bf16[32,2176]{1,0:T(8,128)(2,1)} %concatenate.3.x_ref), custom_call_target="tpu_custom_call" | custom-call | tf_op jit(solution)/shard_map/gather_2/pallas_call | solution.py:144
  91.0 0.0 copy-start.18
  91.0 2.5 %fusion.20 = f32[512,128]{1,0:T(8,128)S(1)} fusion(bf16[2048,128]{1,0:T(8,128)(2,1)} %param.44, bf16[512,2176]{1,0:T(8,128)(2,1)} %bitcast.88), kind=kOutput, calls=%fused_computation.15 | convolution fusion | flops 268435456 | bytes 2883584 | tf_op jit(solution)/shard_map/dot_general | solution.py:285
  93.6 0.0 copy-start.16
  93.6 0.7 fusion.47
  94.3 0.8 fusion.68
  95.1 8.6 %total_3.1 = f32[4,128]{1,0:T(4,128)} custom-call(f32[4,128]{1,0:T(4,128)} %bitcast.96), custom_call_target="tpu_custom_call" | custom-call | tf_op jit(solution)/shard_map/total_3/pallas_call | solution.py:265
  103.7 0.7 divide_bitcast_fusion
  104.4 0.2 fusion.57
  104.6 0.1 reshape.129
  104.7 0.2 reduce_window_sum.11
  104.9 0.1 add_add_fusion
  105.0 0.1 add.122
  105.1 0.7 convolution_convert_fusion.1
  105.8 0.1 select_reduce_fusion
  106.0 3.6 %fusion.26 = f32[256,1024]{1,0:T(8,128)S(1)} fusion(bf16[256,2048]{1,0:T(8,128)(2,1)S(1)} %convolution_convert_fusion.1, bf16[1,2048,1024]{2,1,0:T(8,128)(2,1)} %param.41), kind=kOutput, calls=%fused_computation.19 | convolution fusion | flops 1074003968 | bytes 6291456 | tf_op jit(solution)/shard_map/dot_general | solution.py:68
  109.6 1.5 fusion.41
  111.1 5.9 %fusion.24 = f32[512,2048]{1,0:T(8,128)} fusion(bf16[256,1024]{1,0:T(8,128)(2,1)S(1)} %fusion.41, bf16[1,1024,2048]{2,1,0:T(8,128)(2,1)} %param.43, f32[256]{0:T(256)S(1)} %select_reduce_fusion, s32[512]{0:T(512)S(1)} %broadcast_select_fusion), kind=kOutput, calls=%fused_computation.18 | convolution fusion | flops 1612840960 | bytes 8915968 | tf_op jit(solution)/shard_map/dot_general | solution.py:373
  117.0 4.2 %add_convert_fusion = bf16[512,2048]{1,0:T(8,128)(2,1)} fusion(f32[512,2048]{1,0:T(8,128)} %fusion.24, bf16[512,128]{1,0:T(8,128)(2,1)S(1)} %fusion.47, bf16[128,2048]{1,0:T(8,128)(2,1)S(1)} %copy-done, f32[512]{0:T(512)S(1)} %divide_bitcast_fusion), kind=kOutput, calls=%fused_computation.6 | convolution fusion | flops 271581184 | bytes 6948864 | tf_op jit(solution)/shard_map/dot_general | solution.py:355
  121.2 24.3 %scatter_4.1 = f32[32,2048]{1,0:T(8,128)} custom-call(bf16[16,32,2048]{2,1,0:T(8,128)(2,1)} %bitcast.86), custom_call_target="tpu_custom_call" | custom-call | tf_op jit(solution)/shard_map/scatter_4/pallas_call | solution.py:222
  145.6 1.6 %add_convert_fusion.1 = bf16[32,2048]{1,0:T(8,128)(2,1)} fusion(f32[32,2048]{1,0:T(8,128)} %scatter_4.1, f32[32,2048]{1,0:T(8,128)S(1)} %copy-done.1, bf16[32,2048]{1,0:T(8,128)(2,1)S(1)} %copy-done.2), kind=kLoop, calls=%fused_computation.48 | loop fusion | flops 262144 | bytes 786432 | tf_op jit(solution)/shard_map/convert_element_type | solution.py:375
  (39 shorter events, 0.1 us)
Async XLA Ops:
  0.6 116.4 %copy-start = (bf16[128,2048]{1,0:T(8,128)(2,1)S(1)}, bf16[128,2048]{1,0:T(8,128)(2,1)}, u32[]{:S(2)}) copy-start(bf16[128,2048]{1,0:T(8,128)(2,1)} %param.46) | copy-start | bytes 1572868
  0.6 32.4 %copy-start.8 = (bf16[2048,64]{0,1:T(8,128)(2,1)S(1)}, bf16[2048,64]{0,1:T(8,128)(2,1)}, u32[]{:S(2)}) copy-start(bf16[2048,64]{0,1:T(8,128)(2,1)} %param.30) | copy-start | bytes 786436
  7.2 28.2 %copy-start.11 = (f32[4,64,16]{1,2,0:T(8,128)S(1)}, f32[4,64,16]{1,2,0:T(8,128)}, u32[]{:S(2)}) copy-start(f32[4,64,16]{1,2,0:T(8,128)} %param.35) | copy-start | bytes 49156
  7.2 28.6 %copy-start.6 = (f32[512,4,64]{0,2,1:T(8,128)S(1)}, f32[512,4,64]{0,2,1:T(8,128)}, u32[]{:S(2)}) copy-start(f32[512,4,64]{0,2,1:T(8,128)} %param.27) | copy-start | bytes 1572868
  7.2 28.6 %copy-start.7 = (f32[512,4,64]{0,2,1:T(8,128)S(1)}, f32[512,4,64]{0,2,1:T(8,128)}, u32[]{:S(2)}) copy-start(f32[512,4,64]{0,2,1:T(8,128)} %param.28) | copy-start | bytes 1572868
  7.2 28.6 %copy-start.10 = (f32[4,64,16]{1,2,0:T(8,128)S(1)}, f32[4,64,16]{1,2,0:T(8,128)}, u32[]{:S(2)}) copy-start(f32[4,64,16]{1,2,0:T(8,128)} %param.34) | copy-start | bytes 49156
  35.4 1.1 copy-start.13
  35.4 1.5 %copy-start.12 = (f32[4,16,64]{2,1,0:T(8,128)S(1)}, f32[4,16,64]{2,1,0:T(8,128)}, u32[]{:S(2)}) copy-start(f32[4,16,64]{2,1,0:T(8,128)} %param.37) | copy-start | bytes 49156
  35.4 1.5 %copy-start.15 = (f32[4,16]{1,0:T(4,128)S(1)}, f32[4,16]{1,0:T(4,128)}, u32[]{:S(2)}) copy-start(f32[4,16]{1,0:T(4,128)} %param.38) | copy-start | bytes 772
  35.8 1.6 %copy-start.9 = (bf16[64,2048]{1,0:T(8,128)(2,1)S(1)}, bf16[64,2048]{1,0:T(8,128)(2,1)}, u32[]{:S(2)}) copy-start(bf16[64,2048]{1,0:T(8,128)(2,1)} %param.39) | copy-start | bytes 786436
  36.4 0.9 copy-start.4
  36.4 1.0 copy-start.5
  37.4 27.2 %copy-start.2 = (bf16[32,2048]{1,0:T(8,128)(2,1)S(1)}, bf16[32,2048]{1,0:T(8,128)(2,1)}, u32[]{:S(2)}) copy-start(bf16[32,2048]{1,0:T(8,128)(2,1)} %param.24) | copy-start | bytes 393220
  37.4 28.3 %copy-start.14 = (f32[2048]{0:T(1024)S(1)}, f32[2048]{0:T(1024)}, u32[]{:S(2)}) copy-start(f32[2048]{0:T(1024)} %param.40) | copy-start | bytes 24580
  91.0 2.6 %copy-start.3 = (bf16[16,32,2176]{2,1,0:T(8,128)(2,1)S(1)}, bf16[16,32,2176]{2,1,0:T(8,128)(2,1)}, u32[]{:S(2)}) copy-start(bf16[16,32,2176]{2,1,0:T(8,128)(2,1)} %gather_2.1) | copy-start | bytes 6684676
  91.0 2.6 %copy-start.18 = (bf16[2048,128]{1,0:T(8,128)(2,1)S(1)}, bf16[2048,128]{1,0:T(8,128)(2,1)}, u32[]{:S(2)}) copy-start(bf16[2048,128]{1,0:T(8,128)(2,1)} %param.45) | copy-start | bytes 1572868
  93.6 0.7 copy-start.16
  105.9 3.6 %copy-start.17 = (bf16[1,2048,1024]{2,1,0:T(8,128)(2,1)S(1)}, bf16[1,2048,1024]{2,1,0:T(8,128)(2,1)}, u32[]{:S(2)}) copy-start(bf16[1,2048,1024]{2,1,0:T(8,128)(2,1)} %param.42) | copy-start | bytes 12582916
  121.2 24.4 %copy-start.1 = (f32[32,2048]{1,0:T(8,128)S(1)}, f32[32,2048]{1,0:T(8,128)}, u32[]{:S(2)}) copy-start(f32[32,2048]{1,0:T(8,128)} %scatter_1.1) | copy-start | bytes 786436

commit v2 on v0

--- a/solution.py
+++ b/solution.py
@@ -1,6 +1,10 @@
+import functools
+
 import jax
 import jax.numpy as jnp
 from jax import lax
+from jax.experimental import pallas as pl
+from jax.experimental.pallas import tpu as pltpu
 from jax.sharding import PartitionSpec as P
 
 EPS = 1e-06
@@ -69,6 +73,440 @@
     return jnp.dot(activated, down_weight, preferred_element_type=jnp.float32).astype(jnp.bfloat16)
 
 
+def spot(n):
+    me = lax.axis_index("ep")
+    return me, me // 4, (me // 2) % 2, me % 2, n // 4
+
+
+def index_of(hi, mid, lo):
+    return hi * 4 + mid * 2 + lo
+
+
+def greet(peers, work=lambda: None):
+    barrier = pltpu.get_barrier_semaphore()
+    for peer in peers:
+        pl.semaphore_signal(
+            barrier, inc=1, device_id={"ep": peer}, device_id_type=pl.DeviceIdType.MESH
+        )
+    result = work()
+    pl.semaphore_wait(barrier, len(peers))
+    return result
+
+
+def remote(src, dst, send_sem, recv_sem, peer):
+    return pltpu.make_async_remote_copy(
+        src_ref=src,
+        dst_ref=dst,
+        send_sem=send_sem,
+        recv_sem=recv_sem,
+        device_id={"ep": peer},
+        device_id_type=pl.DeviceIdType.MESH,
+    )
+
+
+class Lane:
+    def __init__(self, send_sem, recv_sem):
+        self.send_sem, self.recv_sem, self.copies = send_sem, recv_sem, []
+
+    def push(self, src, dst, peer):
+        at = len(self.copies)
+        copy = remote(src, dst, self.send_sem.at[at], self.recv_sem.at[at], peer)
+        copy.start()
+        self.copies.append(copy)
+        return copy
+
+    def finish(self):
+        for copy in self.copies:
+            copy.wait_send()
+
+
+def ring_rows(step, limit, way, rows):
+    if step < limit:
+        return pl.ds(0, rows)
+    return pl.ds(0, rows // 2) if way == 1 else pl.ds(rows // 2, rows - rows // 2)
+
+
+def neighbours(n):
+    me, hi, mid, lo, span = spot(n)
+    return [
+        index_of(hi, mid, 1 - lo),
+        index_of(hi, 1 - mid, lo),
+        index_of((hi + 1) % span, mid, lo),
+        index_of((hi + span - 1) % span, mid, lo),
+    ]
+
+
+def spread(n, lane, x, o):
+    me, hi, mid, lo, span = spot(n)
+    core, across, right, left = neighbours(n)
+    ways = {1: right, -1: left}
+    rows, width = x.shape
+    limit = span // 2
+    cut = width // 256 * 128
+    first, second = pl.ds(0, cut), pl.ds(cut, width - cut)
+    whole, full = pl.ds(0, width), pl.ds(0, rows)
+    ends = []
+
+    def relay(slot, at_rows, at_columns, peer):
+        part = o.at[slot, at_rows, at_columns]
+        return lane.push(part, part, peer)
+
+    partner = lane.push(x.at[:, second], o.at[me, :, second], across)
+    own = {way: lane.push(x, o.at[me], peer) for way, peer in ways.items()}
+    crossed = [
+        (
+            lane.push(x.at[:, first], o.at[me, :, first], across),
+            index_of(hi, 1 - mid, lo),
+            full,
+        )
+    ]
+    ends.append(lane.push(x, o.at[me], core))
+    o[me] = x[...]
+    partner.wait_recv()
+    other = {way: relay(across, full, second, peer) for way, peer in ways.items()}
+    ends.append(relay(across, full, second, core))
+    for step in range(1, limit + 1):
+        for way, peer in ways.items():
+            own[way].wait_recv()
+            h = (hi + span - way * step) % span
+            slot = index_of(h, mid, lo)
+            at_rows = ring_rows(step, limit, way, rows)
+            if step < limit:
+                own[way] = relay(slot, ring_rows(step + 1, limit, way, rows), whole, peer)
+            crossed.append(
+                (relay(slot, at_rows, first, across), index_of(h, 1 - mid, lo), at_rows)
+            )
+            ends.append(relay(slot, at_rows, whole, core))
+        for way, peer in ways.items():
+            other[way].wait_recv()
+            slot = index_of((hi + span - way * step) % span, 1 - mid, lo)
+            at_rows = ring_rows(step, limit, way, rows)
+            if step < limit:
+                other[way] = relay(slot, ring_rows(step + 1, limit, way, rows), second, peer)
+            ends.append(relay(slot, at_rows, second, core))
+    for copy, slot, at_rows in crossed:
+        copy.wait_recv()
+        ends.append(relay(slot, at_rows, first, core))
+    for copy in ends:
+        copy.wait_recv()
+
+
+def reduce_to_own(n, lane, x, c_buf, part, y_buf, ring_buf, last_buf):
+    me, hi, mid, lo, span = spot(n)
+    core, across, right, left = neighbours(n)
+    ways = {1: right, -1: left}
+    rows, width = x.shape[1:]
+    limit = span // 2
+    cut = width // 256 * 128
+    first, second = pl.ds(0, cut), pl.ds(cut, width - cut)
+    order = [limit] + [j for j in range(span) if j not in (0, limit)] + [0]
+
+    def add(slot, at_rows, at_columns, value):
+        here = part[slot, at_rows, at_columns].astype(jnp.float32)
+        part[slot, at_rows, at_columns] = (here + value.astype(jnp.float32)).astype(part.dtype)
+
+    def send_on(base, target, way, at_columns, stream):
+        at_rows = ring_rows(target, limit, way, rows)
+        slot = base + (target if way == 1 else (span - target) % span)
+        at = (0 if way == 1 else limit) + limit - target
+        return lane.push(
+            part.at[slot, at_rows, at_columns],
+            ring_buf.at[stream, at, at_rows, at_columns],
+            ways[way],
+        )
+
+    def take(base, target, way, at_columns, stream):
+        at_rows = ring_rows(target + 1, limit, way, rows)
+        slot = base + (target if way == 1 else (span - target) % span)
+        at = (0 if way == 1 else limit) + limit - target - 1
+        add(slot, at_rows, at_columns, ring_buf[stream, at, at_rows, at_columns])
+
+    arrivals = {}
+    for base, side in ((span, 1 - mid), (0, mid)):
+        for j in order:
+            block = x.at[index_of((hi + j) % span, side, 1 - lo)]
+            arrivals[base + j] = lane.push(block, c_buf.at[base + j], core)
+
+    def settle(base, side, j):
+        arrivals[base + j].wait_recv()
+        own = x[index_of((hi + j) % span, side, lo)].astype(jnp.float32)
+        part[base + j] = (own + c_buf[base + j].astype(jnp.float32)).astype(part.dtype)
+
+    chains, crossed = {}, {}
+    for j in order:
+        settle(span, 1 - mid, j)
+        if j == limit:
+            for way in ways:
+                chains[0, way] = send_on(span, limit, way, second, 0)
+        crossed[j] = lane.push(part.at[span + j, :, first], y_buf.at[j, :, first], across)
+    for j in order:
+        settle(0, mid, j)
+        if j == limit:
+            for way in ways:
+                chains[1, way] = send_on(0, limit, way, second, 1)
+
+    def advance(stream, base, at_columns, target):
+        for way in ways:
+            chains[stream, way].wait_recv()
+            take(base, target, way, at_columns, stream)
+            if target > 0:
+                chains[stream, way] = send_on(base, target, way, at_columns, stream)
+
+    def join(j):
+        crossed[j].wait_recv()
+        add(j, pl.ds(0, rows), first, y_buf[j, :, first])
+
+    join(limit)
+    for way in ways:
+        chains[2, way] = send_on(0, limit, way, first, 2)
+    for target in range(limit - 1, -1, -1):
+        advance(0, span, second, target)
+        if target == 0:
+            last = lane.push(part.at[span, :, second], last_buf.at[:, second], across)
+        advance(1, 0, second, target)
+        for j in sorted({target, (span - target) % span}):
+            join(j)
+        advance(2, 0, first, target)
+    last.wait_recv()
+    add(0, pl.ds(0, rows), second, last_buf[:, second])
+
+
+def lane_sems(n):
+    return [pltpu.SemaphoreType.DMA((16 * n,)), pltpu.SemaphoreType.DMA((16 * n,))]
+
+
+def reduce_scratch(n, block, dtype):
+    span = n // 4
+    return [
+        pltpu.VMEM((2 * span,) + block, dtype),
+        pltpu.VMEM((2 * span,) + block, dtype),
+        pltpu.VMEM((span,) + block, dtype),
+        pltpu.VMEM((3, span) + block, dtype),
+        pltpu.VMEM(block, dtype),
+    ]
+
+
+def vmem_specs(count):
+    return [pl.BlockSpec(memory_space=pltpu.VMEM)] * count
+
+
+def arrival_order(span):
+    return sorted(range(span - 1), key=lambda j: min(j + 1, span - 1 - j))
+
+
+def spread_simple(n, lane, x, o):
+    me, hi, mid, lo, span = spot(n)
+    core, across, right, left = neighbours(n)
+    ahead = [(hi + 1 + j) % span for j in range(span - 1)]
+    behind = [(hi + span - 1 - j) % span for j in range(span - 1)]
+
+    def relay(slot, peer):
+        return lane.push(o.at[slot], o.at[slot], peer)
+
+    z_copies = [lane.push(x, o.at[me], index_of(h, mid, lo)) for h in ahead]
+    y_copies = [lane.push(x, o.at[me], across)]
+    ends = [lane.push(x, o.at[me], core)]
+    o[me] = x[...]
+    for j in arrival_order(span):
+        z_copies[j].wait_recv()
+        slot = index_of(behind[j], mid, lo)
+        y_copies.append(relay(slot, across))
+        ends.append(relay(slot, core))
+    slots = [hi] + [behind[j] for j in arrival_order(span)]
+    for j in range(span):
+        y_copies[j].wait_recv()
+        ends.append(relay(index_of(slots[j], 1 - mid, lo), core))
+    for copy in ends:
+        copy.wait_recv()
+
+
+def units_kernel(n, tokens_ref, gain_ref, weight_ref, o_ref, row_buf, all_buf, *sems):
+    def norm():
+        row_buf[...] = rms_scale(tokens_ref[...].astype(jnp.float32), gain_ref[...]).astype(
+            row_buf.dtype
+        )
+
+    rows, width = tokens_ref.shape
+    me, hi, mid, lo, span = spot(n)
+    columns = [index_of((hi + 1 + j) % span, mid, lo) for j in range(span - 1)]
+    core, across, right, left = neighbours(n)
+    greet([core, across] + columns, norm)
+    lane = Lane(*sems)
+    spread_simple(n, lane, row_buf, all_buf)
+    for i in range(4):
+        part = n // 4
+        here = all_buf[i * part : (i + 1) * part].reshape(part * rows, width)
+        o_ref[:, i * part * rows : (i + 1) * part * rows] = lax.dot_general(
+            weight_ref[...],
+            here,
+            (((1,), (1,)), ((), ())),
+            preferred_element_type=jnp.float32,
+        ).astype(o_ref.dtype)
+    lane.finish()
+
+
+def gather_units(tokens, gain, weight, n, collective_id):
+    rows, width = tokens.shape
+    return pl.pallas_call(
+        functools.partial(units_kernel, n),
+        out_shape=jax.ShapeDtypeStruct((weight.shape[1], n * rows), jnp.bfloat16),
+        in_specs=vmem_specs(3),
+        out_specs=vmem_specs(1)[0],
+        scratch_shapes=[
+            pltpu.VMEM((rows, width), jnp.bfloat16),
+            pltpu.VMEM((n, rows, width), jnp.bfloat16),
+        ]
+        + lane_sems(n),
+        compiler_params=pltpu.CompilerParams(
+            collective_id=collective_id, has_side_effects=True
+        ),
+        name=f"units_{collective_id}",
+    )(tokens, gain.reshape(1, -1), weight.T).T
+
+
+def scatter_kernel(n, x_ref, own_ref, o_ref, c_buf, part, y_buf, ring_buf, last_buf, *sems):
+    greet(neighbours(n))
+    lane = Lane(*sems)
+    reduce_to_own(n, lane, x_ref, c_buf, part, y_buf, ring_buf, last_buf)
+    o_ref[...] = (own_ref[...] + part[0].astype(jnp.float32)).astype(o_ref.dtype)
+    lane.finish()
+
+
+def scatter_rows(x, own, n, collective_id):
+    rows, width = own.shape
+    block = (rows, width)
+    return pl.pallas_call(
+        functools.partial(scatter_kernel, n),
+        out_shape=jax.ShapeDtypeStruct(block, jnp.bfloat16),
+        in_specs=vmem_specs(2),
+        out_specs=vmem_specs(1)[0],
+        scratch_shapes=reduce_scratch(n, block, x.dtype) + lane_sems(n),
+        compiler_params=pltpu.CompilerParams(
+            collective_id=collective_id, has_side_effects=True
+        ),
+        name=f"scatter_{collective_id}",
+    )(x.reshape((n,) + block), own)
+
+
+def middle_kernel(
+    n,
+    x_ref,
+    tokens_ref,
+    gain_ref,
+    routes_ref,
+    scores_ref,
+    gate_ref,
+    up_ref,
+    mix_ref,
+    all_ref,
+    residual_ref,
+    hidden_ref,
+    logit_ref,
+    c_buf,
+    part,
+    y_buf,
+    ring_buf,
+    last_buf,
+    row_buf,
+    logit_own,
+    logit_buf,
+    *sems,
+):
+    me = lax.axis_index("ep")
+    peers = [(me + 1 + j) % n for j in range(n - 1)]
+    rows, width = tokens_ref.shape
+
+    def share_table():
+        weights = jnp.exp(scores_ref[...])
+        weights = weights / jnp.sum(weights, axis=1, keepdims=True)
+        spare = row_buf.shape[1] - width
+        ids = lax.broadcasted_iota(jnp.int32, (rows, spare), 1)
+        expert = ids % n
+        table = jnp.zeros((rows, spare), jnp.float32)
+        for k in range(weights.shape[1]):
+            hit = routes_ref[:, k : k + 1] == expert
+            table = table + jnp.where(hit, weights[:, k : k + 1], 0.0)
+        coarse = table.astype(row_buf.dtype).astype(jnp.float32)
+        value = jnp.where(ids < n, coarse, jnp.where(ids < 2 * n, table - coarse, 0.0))
+        row_buf[:, width:] = value.astype(row_buf.dtype)
+
+    greet(peers, share_table)
+    lane = Lane(*sems)
+    reduce_to_own(n, lane, x_ref, c_buf, part, y_buf, ring_buf, last_buf)
+    residual = tokens_ref[...].astype(jnp.float32) + part[0].astype(jnp.float32)
+    residual_ref[...] = residual
+    row_buf[:, :width] = rms_scale(residual, gain_ref[...]).astype(row_buf.dtype)
+    spread(n, lane, row_buf, all_ref)
+    chunk = 128 // rows
+    total = jnp.zeros(logit_own.shape, jnp.float32)
+    mix_shape = (logit_own.shape[0], mix_ref.shape[1])
+    row_ids = lax.broadcasted_iota(jnp.int32, mix_shape, 0)
+    for i in range(n // chunk):
+        here = all_ref[i * chunk : (i + 1) * chunk, :, :width].reshape(128, width)
+        hidden = dense_hidden(here, gate_ref[...], up_ref[...])
+        hidden_ref[i * 128 : (i + 1) * 128] = hidden
+        chosen = jnp.where(row_ids == i, mix_ref[...], 0.0)
+        total = total + lax.dot_general(
+            chosen,
+            hidden.astype(jnp.float32),
+            (((1,), (1,)), ((), ())),
+            precision=HIGH,
+            preferred_element_type=jnp.float32,
+        )
+    logit_own[...] = total
+    copies = [lane.push(logit_own, logit_buf.at[j], peers[j]) for j in range(n - 1)]
+    for j in range(n - 1):
+        copies[j].wait_recv()
+        total = total + logit_buf[j]
+    logit_ref[...] = total
+    lane.finish()
+
+
+def middle(part, tokens, gain_mid, routes, scores, dense_gate, dense_up, dense_mix, n, collective_id):
+    rows, width = tokens.shape
+    block = (rows, width)
+    wide = width + -(-(2 * n) // 128) * 128
+    units = dense_gate.shape[1]
+    logit_shape = (-(-(n * rows) // 1024) * 8, 128)
+    gathered, residual, hidden, logits = pl.pallas_call(
+        functools.partial(middle_kernel, n),
+        out_shape=[
+            jax.ShapeDtypeStruct((n, rows, wide), jnp.bfloat16),
+            jax.ShapeDtypeStruct(block, jnp.float32),
+            jax.ShapeDtypeStruct((n * rows, units), jnp.bfloat16),
+            jax.ShapeDtypeStruct(logit_shape, jnp.float32),
+        ],
+        in_specs=vmem_specs(8),
+        out_specs=vmem_specs(4),
+        scratch_shapes=reduce_scratch(n, block, part.dtype)
+        + [
+            pltpu.VMEM((rows, wide), jnp.bfloat16),
+            pltpu.VMEM(logit_shape, jnp.float32),
+            pltpu.VMEM((n - 1,) + logit_shape, jnp.float32),
+        ]
+        + lane_sems(n),
+        compiler_params=pltpu.CompilerParams(
+            collective_id=collective_id, has_side_effects=True
+        ),
+        name=f"middle_{collective_id}",
+    )(
+        part.reshape((n,) + block),
+        tokens,
+        gain_mid.reshape(1, -1),
+        routes,
+        scores,
+        dense_gate,
+        dense_up,
+        dense_mix.reshape(1, -1),
+    )
+    return (
+        gathered.reshape(n * rows, wide),
+        residual,
+        hidden,
+        logits.reshape(-1)[: n * rows],
+    )
+
+
 def dense_hidden(row_block, dense_gate, dense_up):
     return (
         jax.nn.silu(jnp.dot(row_block, dense_gate, preferred_element_type=jnp.float32))
@@ -103,17 +541,11 @@
     dense_mix,
 ):
     devices = lax.axis_size("ep")
-    own_rows = tokens.shape[0]
+    me = lax.axis_index("ep")
+    own_rows, width = tokens.shape
     top_count = routes.shape[1]
-    width = tokens.shape[1]
     capacity = max(2, 2 * own_rows * top_count // devices)
-    inputs = tokens.astype(jnp.float32)
-    normed = rms_scale(inputs, gain_in).astype(jnp.bfloat16)
-    unit_rows = jnp.dot(
-        lax.all_gather(normed, "ep", axis=0, tiled=True),
-        proj_in,
-        preferred_element_type=jnp.float32,
-    ).astype(jnp.bfloat16)
+    unit_rows = gather_units(tokens, gain_in, proj_in, devices, 0)
     branch, new_real, new_imag = state_step(
         unit_rows,
         state_real,
@@ -127,48 +559,42 @@
         output_imag,
         skip_gain,
     )
-    whole_out = lax.all_gather(proj_out, "ep", axis=0, tiled=True)
-    own_branch = lax.all_to_all(branch, "ep", split_axis=0, concat_axis=1, tiled=True)
-    mixer_out = jnp.dot(own_branch, whole_out, preferred_element_type=jnp.float32)
-    residual = inputs + mixer_out
-    mixed = rms_scale(residual, gain_mid).astype(jnp.bfloat16)
-    weights = jnp.exp(route_logits)
-    weights = weights / jnp.sum(weights, axis=1, keepdims=True)
-    hidden = dense_hidden(lax.all_gather(mixed, "ep", axis=0, tiled=True), dense_gate, dense_up)
+    mixer_part = jnp.dot(branch, proj_out, preferred_element_type=jnp.float32)
+    expert_ids = jnp.arange(devices, dtype=jnp.int32)
+    gathered, residual, hidden, gate_logit = middle(
+        mixer_part.astype(jnp.bfloat16),
+        tokens,
+        gain_mid,
+        routes,
+        route_logits,
+        dense_gate,
+        dense_up,
+        dense_mix,
+        devices,
+        1,
+    )
+    all_mixed = gathered[:, :width]
     dense_term = jnp.dot(hidden, dense_down, preferred_element_type=jnp.float32)
-    logit_term = jnp.dot(hidden.astype(jnp.float32), dense_mix, precision=HIGH)
-    dense_out, gate_logit = (
-        lax.psum_scatter(
-            dense_term.astype(jnp.bfloat16), "ep", scatter_dimension=0, tiled=True
-        ).astype(jnp.float32),
-        lax.psum_scatter(
-            logit_term.astype(jnp.bfloat16), "ep", scatter_dimension=0, tiled=True
-        ).astype(jnp.float32),
-    )
-    flat_routes = routes.reshape(-1)
-    chosen = (flat_routes[:, None] == jnp.arange(devices, dtype=jnp.int32)[None, :]).astype(
-        jnp.int32
-    )
-    slot_index = jnp.sum((jnp.cumsum(chosen, axis=0) - 1) * chosen, axis=1)
-    position = (flat_routes * capacity + slot_index).reshape(own_rows, top_count)
+    mine = (expert_ids == me)[None, :]
+    extra = gathered[:, width:].astype(jnp.float32)
+    share = jnp.sum(
+        jnp.where(mine, extra[:, :devices] + extra[:, devices : 2 * devices], 0.0), axis=1
+    ).reshape(devices, own_rows)
+    taken = share > 0.0
+    slot = jnp.cumsum(taken.astype(jnp.int32), axis=1) - 1
+    slot = jnp.where(taken, slot + expert_ids[:, None] * capacity, -1).reshape(-1)
     slot_ids = jnp.arange(devices * capacity, dtype=jnp.int32)
-    matches = position[:, :, None] == slot_ids[None, None, :]
-    dispatch = jnp.any(matches, axis=1).astype(jnp.bfloat16)
-    send_buffer = jnp.dot(dispatch.T, mixed, preferred_element_type=jnp.float32).astype(
-        jnp.bfloat16
-    )
-    send_buffer = send_buffer.reshape(devices, capacity, width)
-    received = lax.all_to_all(send_buffer, "ep", split_axis=0, concat_axis=0, tiled=True)
-    flat_rows = received.reshape(-1, width)
+    picks = slot[None, :] == slot_ids[:, None]
+    places = slot[:, None] == slot_ids[None, :]
+    flat_rows = jnp.dot(
+        picks.astype(jnp.bfloat16), all_mixed, preferred_element_type=jnp.float32
+    ).astype(jnp.bfloat16)
     result = expert_apply(flat_rows, expert_gate[0], expert_up[0], expert_down[0])
-    returned = lax.all_to_all(
-        result.reshape(received.shape), "ep", split_axis=0, concat_axis=0, tiled=True
-    )
-    combine = jnp.sum(jnp.where(matches, weights[:, :, None], 0.0), axis=1)
-    routed = jnp.dot(combine, returned.reshape(-1, width).astype(jnp.float32), precision=HIGH)
-    layer_out = (residual + routed + jax.nn.sigmoid(gate_logit)[:, None] * dense_out).astype(
-        jnp.bfloat16
-    )
+    slot_share = jnp.sum(jnp.where(picks, share.reshape(1, -1), 0.0), axis=1, keepdims=True)
+    scaled = (result.astype(jnp.float32) * slot_share).astype(jnp.bfloat16)
+    routed = jnp.dot(places.astype(jnp.bfloat16), scaled, preferred_element_type=jnp.float32)
+    part = (routed + jax.nn.sigmoid(gate_logit)[:, None] * dense_term).astype(jnp.bfloat16)
+    layer_out = scatter_rows(part, residual, devices, 2)
     return (layer_out, new_real, new_imag)
 
 

time: 240 us -> 143 us (0.60)
  waiting for transfers between devices: 120 us -> 0 us
  Pallas kernels: 0 us -> 108 us
  blocking collectives: 58.4 us -> 0 us
  between operations: 14.8 us -> 0.85 us
  starting transfers between devices: 7.47 us -> 0 us
  matrix products: 30.9 us -> 25.4 us
  local copies, waits for them, and re-layouts: 2.64 us -> 5.23 us
    all_gather x3 -> x0, waiting for transfers between devices: 117 us -> none  [the longest x1 42.6 us: on_device(): lax.all_gather(normed, 'ep', axis=0, tiled=True)]
    pallas_call x0 -> x3, Pallas kernels: none -> 108 us  [the longest x1 54.7 us: middle(): pl.pallas_call(functools.partial(middle_kernel, n), out_shape=[jax.ShapeD...]
    unnamed x1 -> x0, blocking collectives: 47 us -> none
    all_to_all x1 -> x0, blocking collectives: 11.5 us -> none  [on_device(): lax.all_to_all(branch, 'ep', split_axis=0, concat_axis=1, tiled=True)]
    dot_general x8 -> x4, matrix products: 22 us -> 12 us  [the longest x1 6.17 us: on_device(): jnp.dot(places.astype(jnp.bfloat16), scaled, preferred_element_type=jnp.f...]
    all_to_all x2 -> x0, starting transfers between devices: 7.31 us -> none  [the longest x1 3.65 us: on_device(): lax.all_to_all(result.reshape(received.shape), 'ep', split_axis=0, concat...]
    unnamed x36 -> x19, local copies, waits for them, and re-layouts: 1.04 us -> 4.34 us
  transfers between devices with their start and end apart: 6 -> 0, of which waited for: 4 -> 0; matrix products, arithmetic and copies ran while one was open for 12% -> 0% of each run, Pallas kernels for 0% -> 0%
where the time goes in v2:
time: 143 us
  Pallas kernels  108 us (76%)
  matrix products  25.4 us (18%)
  local copies, waits for them, and re-layouts  5.23 us (4%)
  other arithmetic  3.09 us (2%)
    pallas_call x1, Pallas kernels, middle(): pl.pallas_call(functools.partial(middle_kernel, n), out_shape=[jax.ShapeD...  54.7 us
    pallas_call x1, Pallas kernels, gather_units(): pl.pallas_call(functools.partial(units_kernel, n), out_shape=jax.ShapeDty...  27.9 us
    pallas_call x1, Pallas kernels, scatter_rows(): pl.pallas_call(functools.partial(scatter_kernel, n), out_shape=jax.ShapeD...  25.7 us
    dot_general x1, matrix products, on_device(): jnp.dot(places.astype(jnp.bfloat16), scaled, preferred_element_type=jnp.f...  6.17 us
    unnamed x19, local copies, waits for them, and re-layouts  4.34 us
    dot_general x1, matrix products, on_device(): dense_term = jnp.dot(hidden, dense_down, preferred_element_type=jnp.float32)  4.2 us
    dot_general x1, matrix products, expert_apply(): jnp.dot(row_block, gate_weight, preferred_element_type=jnp.float32)  3.62 us

profile of v2, /device:TPU:0, one launch (start us, length us, event | category | flops | bytes accessed | tf_op | source)
XLA Modules:
  0.0 142.8 jit_solution(5144013988880950006)
XLA Ops:
  0.6 0.0 copy-start
  0.6 0.0 copy-start.3
  0.7 0.0 copy-start.6
  0.7 0.0 copy-start.5
  0.7 0.7 exp.17
  1.4 0.8 cosine_multiply_fusion
  2.2 1.4 copy.29.routes_ref
  3.6 1.4 copy.30.scores_ref
  5.0 27.9 %units_0.1 = bf16[64,512]{1,0:T(8,128)(2,1)} custom-call(bf16[32,2048]{1,0:T(8,128)(2,1)} %tokens_ref.3, f32[1,2048]{1,0:T(1,128)} %bitcast.86, bf16[64,2048]{1,0:T(8,128)(2,1)} %bitcast.85), custom_call_target="tpu_custom_call" | custom-call | tf_op jit(solution)/shard_map/units_0/pallas_call | solution.py:350
  32.9 1.2 fusion.56
  34.1 1.9 %bitcast_add_fusion = (f32[512,4,64]{0,2,1:T(8,128)S(1)}, f32[512,4,64]{0,2,1:T(8,128)S(1)}) fusion(f32[4,512,64]{1,2,0:T(8,128)S(1)} %fusion.56, f32[512,4,64]{0,2,1:T(8,128)} %param.27, f32[512,4,64]{0,2,1:T(8,128)} %param.28, f32[4,64]{1,0:T(4,128)S(1)} %get-tuple-element.17, f32[4,64]{1,0:T(4,128)S(1)} %get-tuple-element.16, ...), kind=kOutput, calls=%fused_computation.25 | convolution fusion | flops 27000832 | bytes 2707456 | tf_op jit(solution)/shard_map/sgp,gnp->sgn/dot_general | solution.py:44
  36.0 0.0 copy-start.1
  36.0 0.0 copy-start.2
  36.0 1.2 fusion.57
  37.2 0.0 copy-done.6
  37.2 0.0 copy-done.5
  37.3 1.3 fusion.54
  38.5 0.0 copy-done.3
  38.5 2.0 %convolution_convert_fusion = bf16[512,2048]{1,0:T(8,128)(2,1)} fusion(bf16[512,64]{0,1:T(8,128)(2,1)S(1)} %bitcast.84, bf16[64,2048]{1,0:T(8,128)(2,1)S(1)} %copy-done.3), kind=kOutput, calls=%fused_computation.7 | convolution fusion | flops 135266304 | bytes 2424832 | tf_op jit(solution)/shard_map/dot_general | solution.py:562
  40.6 54.7 %middle_1.1 = (bf16[16,32,2176]{2,1,0:T(8,128)(2,1)}, f32[32,2048]{1,0:T(8,128)}, bf16[512,128]{1,0:T(8,128)(2,1)}, f32[8,128]{1,0:T(8,128)}) custom-call(bf16[16,32,2048]{2,1,0:T(8,128)(2,1)} %bitcast.79, bf16[32,2048]{1,0:T(8,128)(2,1)} %tokens_ref.3, f32[1,2048]{1,0:T(1,128)} %bitcast.87, s32[32,4]{1,0:T(8,128)} %copy.29.routes_ref, ...), custom_call_target="tpu_custom_call" | custom-call | tf_op jit(solution)/shard_map/middle_1/pallas_call | solution.py:471
  95.3 0.7 divide_bitcast_fusion
  95.9 0.9 slice_convert_fusion
  96.9 0.2 fusion.44
  97.1 0.1 reshape.113
  97.2 0.2 reduce_window_sum.11
  97.4 0.1 add_add_fusion
  97.5 0.1 add.93
  97.6 2.3 %convolution_convert_fusion.1 = bf16[256,2048]{1,0:T(8,128)(2,1)S(1)} fusion(bf16[512,2176]{1,0:T(8,128)(2,1)} %bitcast.89, s32[512]{0:T(512)S(1)} %broadcast_select_fusion), kind=kOutput, calls=%fused_computation.8 | convolution fusion | flops 537526272 | bytes 3147776 | tf_op jit(solution)/shard_map/dot_general | solution.py:589
  99.9 0.0 copy-done.1
  99.9 0.0 copy-done.2
  99.9 0.0 copy-start.7
  99.9 0.1 select_reduce_fusion
  100.0 3.6 %fusion.22 = f32[256,1024]{1,0:T(8,128)S(1)} fusion(bf16[256,2048]{1,0:T(8,128)(2,1)S(1)} %convolution_convert_fusion.1, bf16[1,2048,1024]{2,1,0:T(8,128)(2,1)} %param.41), kind=kOutput, calls=%fused_computation.15 | convolution fusion | flops 1074003968 | bytes 6291456 | tf_op jit(solution)/shard_map/dot_general | solution.py:68
  103.7 0.0 copy-done.7
  103.7 1.4 %fusion.37 = bf16[256,1024]{1,0:T(8,128)(2,1)S(1)} fusion(f32[256,1024]{1,0:T(8,128)S(1)} %fusion.22, bf16[256,2048]{1,0:T(8,128)(2,1)S(1)} %convolution_convert_fusion.1, bf16[1,2048,1024]{2,1,0:T(8,128)(2,1)S(1)} %copy-done.7), kind=kOutput, calls=%fused_computation.20 | convolution fusion | flops 1076101120 | bytes 6815744 | tf_op jit(solution)/shard_map/dot_general | solution.py:70
  105.1 0.0 copy-start.4
  105.1 6.2 %fusion.20 = f32[512,2048]{1,0:T(8,128)} fusion(bf16[256,1024]{1,0:T(8,128)(2,1)S(1)} %fusion.37, bf16[1,1024,2048]{2,1,0:T(8,128)(2,1)} %param.43, f32[256]{0:T(256)S(1)} %select_reduce_fusion, s32[512]{0:T(512)S(1)} %broadcast_select_fusion), kind=kOutput, calls=%fused_computation.14 | convolution fusion | flops 1612840960 | bytes 8915968 | tf_op jit(solution)/shard_map/dot_general | solution.py:595
  111.3 0.0 copy-done
  111.3 0.0 copy-done.4
  111.3 4.2 %add_convert_fusion = bf16[512,2048]{1,0:T(8,128)(2,1)} fusion(f32[512,2048]{1,0:T(8,128)} %fusion.20, bf16[512,128]{1,0:T(8,128)(2,1)S(1)} %copy-done.4, bf16[128,2048]{1,0:T(8,128)(2,1)S(1)} %copy-done, f32[512]{0:T(512)S(1)} %divide_bitcast_fusion), kind=kOutput, calls=%fused_computation.6 | convolution fusion | flops 271581184 | bytes 6948864 | tf_op jit(solution)/shard_map/dot_general | solution.py:577
  115.5 25.7 %scatter_2.1 = bf16[32,2048]{1,0:T(8,128)(2,1)} custom-call(bf16[16,32,2048]{2,1,0:T(8,128)(2,1)} %bitcast.80, f32[32,2048]{1,0:T(8,128)} %get-tuple-element.10.own_ref), custom_call_target="tpu_custom_call" | custom-call | tf_op jit(solution)/shard_map/scatter_2/pallas_call | solution.py:378
  141.2 1.6 %copy.32 = bf16[32,2048]{1,0:T(8,128)(2,1)} copy(bf16[32,2048]{1,0:T(8,128)(2,1)} %scatter_2.1) | data formatting | bytes 262144
  (4 shorter events, 0.0 us)
Async XLA Ops:
  0.6 110.7 %copy-start = (bf16[128,2048]{1,0:T(8,128)(2,1)S(1)}, bf16[128,2048]{1,0:T(8,128)(2,1)}, u32[]{:S(2)}) copy-start(bf16[128,2048]{1,0:T(8,128)(2,1)} %param.46) | copy-start | bytes 1572868
  0.6 37.9 %copy-start.3 = (bf16[64,2048]{1,0:T(8,128)(2,1)S(1)}, bf16[64,2048]{1,0:T(8,128)(2,1)}, u32[]{:S(2)}) copy-start(bf16[64,2048]{1,0:T(8,128)(2,1)} %param.39) | copy-start | bytes 786436
  0.7 36.6 %copy-start.6 = (f32[4,16]{1,0:T(4,128)S(1)}, f32[4,16]{1,0:T(4,128)}, u32[]{:S(2)}) copy-start(f32[4,16]{1,0:T(4,128)} %param.38) | copy-start | bytes 772
  0.7 36.6 %copy-start.5 = (f32[4,16,64]{2,1,0:T(8,128)S(1)}, f32[4,16,64]{2,1,0:T(8,128)}, u32[]{:S(2)}) copy-start(f32[4,16,64]{2,1,0:T(8,128)} %param.37) | copy-start | bytes 49156
  36.0 63.9 %copy-start.1 = (f32[512,4,64]{0,2,1:T(8,128)}, f32[512,4,64]{0,2,1:T(8,128)S(1)}, u32[]{:S(2)}) copy-start(f32[512,4,64]{0,2,1:T(8,128)S(1)} %get-tuple-element.24) | copy-start | bytes 1572868
  36.0 63.9 %copy-start.2 = (f32[512,4,64]{0,2,1:T(8,128)}, f32[512,4,64]{0,2,1:T(8,128)S(1)}, u32[]{:S(2)}) copy-start(f32[512,4,64]{0,2,1:T(8,128)S(1)} %get-tuple-element.23) | copy-start | bytes 1572868
  99.9 3.8 %copy-start.7 = (bf16[1,2048,1024]{2,1,0:T(8,128)(2,1)S(1)}, bf16[1,2048,1024]{2,1,0:T(8,128)(2,1)}, u32[]{:S(2)}) copy-start(bf16[1,2048,1024]{2,1,0:T(8,128)(2,1)} %param.42) | copy-start | bytes 12582916
  105.1 6.2 %copy-start.4 = (bf16[512,128]{1,0:T(8,128)(2,1)S(1)}, bf16[512,128]{1,0:T(8,128)(2,1)}, u32[]{:S(2)}) copy-start(bf16[512,128]{1,0:T(8,128)(2,1)} %get-tuple-element.9) | copy-start | bytes 393220
